TPU v7x, 32 devices: a whole 2x2x4 slice. The times are simulated.
32 devices in a mesh: grp: 2 (over y), row: 4 (over z), col: 4 (over x, core).
Axes of the slice: x: 2, y: 2, z: 4, core: 2. Of those that a mesh axis runs over, the one named last changes fastest.
Arguments:
- tokens: bfloat16 [5120, 2048], P(('grp', 'row')), parts along dimension 0, may hold values from -6 to 6
- w_four: bfloat16 [2048, 1024], P(None, 'col'), may hold values from -0.125 to 0.125
- w_gate: bfloat16 [2048, 2048], P(None, 'col'), may hold values from -0.125 to 0.125
- w_back: bfloat16 [1024, 2048], P(None, 'col'), may hold values from -0.1875 to 0.1875
Outputs:
- mixed: bfloat16 [5120, 2048], P(('grp', 'row'), 'col'), parts along dimension 0
There are 2 independent parts, one for each index of `grp`. A program takes and returns all parts, laid end to end along the dimension named above; an argument that names none is the same for every part. Nothing has to cross between parts.
All inputs are finite; a program needn't handle non-finite values.
Results may differ from a plain program's by a relative error of at most 0.0085.
Values may be sent and summed in bfloat16 or wider, within the bound.
A program may use at most 64 MiB of HBM per device.

v0:
```python
import math

import jax
import jax.numpy as jnp
from jax import lax
from jax.sharding import PartitionSpec as P

GROUP_DIM = 128


def tables(count_len):
    steps = lax.iota(jnp.int32, count_len)
    product = steps[:, None] * steps[None, :] % count_len
    angles = product.astype(jnp.float32) * (2.0 * math.pi / count_len)
    return (jnp.cos(angles), jnp.sin(angles))


def channel_mix(values, matrix):
    height = values.shape[0]
    shaped = values.reshape(height, -1, GROUP_DIM)
    mixed_ch = jnp.einsum("ngc,cj->ngj", shaped, matrix, precision=lax.Precision.HIGHEST)
    return mixed_ch.reshape(height, -1)


def across_rows(values, matrix):
    return jnp.einsum("kr,rmc->kmc", matrix, values, precision=lax.Precision.HIGHEST)


def long_transform(col_re, col_im):
    length = col_re.shape[0]
    first_len = 8
    second_len = length // first_len
    shaped_re = col_re.reshape(first_len, second_len, -1)
    shaped_im = col_im.reshape(first_len, second_len, -1)
    cos_first, sin_first = tables(first_len)
    cos_second, sin_second = tables(second_len)
    section_re = across_rows(shaped_re, cos_first) + across_rows(shaped_im, sin_first)
    section_im = across_rows(shaped_im, cos_first) - across_rows(shaped_re, sin_first)
    outer = lax.iota(jnp.int32, first_len)[:, None]
    inner = lax.iota(jnp.int32, second_len)[None, :]
    angle = (outer * inner % length).astype(jnp.float32) * (2.0 * math.pi / length)
    turn_cos = jnp.cos(angle)[:, :, None]
    turn_sin = jnp.sin(angle)[:, :, None]
    bent_re = section_re * turn_cos + section_im * turn_sin
    bent_im = section_im * turn_cos - section_re * turn_sin
    final_re = jnp.einsum("qb,kbc->qkc", cos_second, bent_re, precision=lax.Precision.HIGHEST)
    final_re = final_re + jnp.einsum(
        "qb,kbc->qkc", sin_second, bent_im, precision=lax.Precision.HIGHEST
    )
    final_re = final_re.reshape(length, -1)
    final_im = jnp.einsum("qb,kbc->qkc", cos_second, bent_im, precision=lax.Precision.HIGHEST)
    final_im = final_im - jnp.einsum(
        "qb,kbc->qkc", sin_second, bent_re, precision=lax.Precision.HIGHEST
    )
    return (final_re, final_im.reshape(length, -1))


def on_device(tokens, w_four, w_gate, w_back):
    length = tokens.shape[0]
    row_count = lax.axis_size("row")
    row_index = lax.axis_index("row")
    piece_rows = length // row_count
    total_len = length * row_count
    feats = jnp.dot(tokens, w_four, preferred_element_type=jnp.float32).astype(jnp.bfloat16)
    lifted = feats.astype(jnp.float32)
    cos_group, sin_group = tables(GROUP_DIM)
    cos_rows, sin_rows = tables(row_count)
    residue = lax.iota(jnp.int32, row_count)[:, None]
    within = row_index * piece_rows + lax.iota(jnp.int32, piece_rows)[None, :]
    twist = (residue * within % total_len).astype(jnp.float32) * (2.0 * math.pi / total_len)
    twist_cos = jnp.cos(twist)[:, :, None]
    twist_sin = jnp.sin(twist)[:, :, None]
    line_re = lax.all_to_all(
        lifted[None].astype(jnp.bfloat16), "row", split_axis=1, concat_axis=0, tiled=True
    ).astype(jnp.float32)
    freq_re = across_rows(line_re, cos_rows)
    freq_im = -across_rows(line_re, sin_rows)
    turned_re = freq_re * twist_cos + freq_im * twist_sin
    turned_im = freq_im * twist_cos - freq_re * twist_sin
    col_re, col_im = (
        lax.all_to_all(turned_re, "row", split_axis=0, concat_axis=1, tiled=True),
        lax.all_to_all(turned_im, "row", split_axis=0, concat_axis=1, tiled=True),
    )
    col_re = col_re.reshape(length, -1)
    col_im = col_im.reshape(length, -1)
    whole_re, whole_im = long_transform(col_re, col_im)
    result = channel_mix(whole_re, cos_group) + channel_mix(whole_im, sin_group)
    scaled = (result * (1.0 / math.sqrt(total_len * GROUP_DIM))).astype(jnp.bfloat16)
    ordered = lax.all_to_all(scaled[:, None], "row", split_axis=0, concat_axis=1, tiled=True)
    ordered = ordered.reshape(length, -1)
    proj = jnp.dot(
        lax.all_gather(ordered, "col", axis=1, tiled=True),
        w_back,
        preferred_element_type=jnp.float32,
    )
    gate = jax.nn.sigmoid(jnp.dot(tokens, w_gate, preferred_element_type=jnp.float32))
    return (gate * proj).astype(jnp.bfloat16)


def solution(mesh):
    return jax.shard_map(
        on_device,
        mesh=mesh,
        in_specs=(P(("grp", "row"), None), P(None, "col"), P(None, "col"), P(None, "col")),
        out_specs=P(("grp", "row"), "col"),
        check_vma=False,
    )
```

profile of v0, /device:TPU:0, one launch (start us, length us, event | category | flops | bytes accessed | tf_op | source)
XLA Modules:
  0.0 142.1 jit_solution(10061951131345919692)
XLA Ops:
  6.5 1.7 %copy-done = bf16[640,2048]{1,0:T(8,128)(2,1)S(1)} copy-done((bf16[640,2048]{1,0:T(8,128)(2,1)S(1)}, bf16[640,2048]{1,0:T(8,128)(2,1)}, u32[]{:S(2)}) %copy-start) | copy-done | bytes 2621464
  8.3 2.1 %fusion.6 = bf16[1,640,256]{2,1,0:T(8,128)(2,1)S(1)} fusion(bf16[640,2048]{1,0:T(8,128)(2,1)S(1)} %copy-done, bf16[2048,256]{1,0:T(8,128)(2,1)} %param.5), kind=kOutput, calls=%fused_computation.15 | convolution fusion | flops 671252480 | bytes 3997696 | tf_op jit(solution)/shard_map/dot_general | solution.py:64
  10.3 0.5 copy.119
  10.9 0.6 broadcast.193
  11.4 3.3 %reduce = bf16[640,256]{1,0:T(8,128)(2,1)} reduce(bf16[640,1,256]{2,1,0:T(2,128)(2,1)S(1)} %bitcast.61, bf16[]{:T(256)} %broadcast.193), dimensions={1}, to_apply=%bitcast.56.reduce_sub_computation | reduce | bytes 655362
  14.7 1.8 %reshape.136 = bf16[4,2,20480]{2,1,0:T(2,128)(2,1)} reshape(bf16[640,256]{1,0:T(8,128)(2,1)} %reduce) | data formatting | bytes 655360
  16.5 6.3 %all-to-all-start = ((bf16[4,2,20480]{2,1,0:T(2,128)(2,1)}), bf16[4,2,20480]{2,1,0:T(2,128)(2,1)}, u32[]{:S(2)}, u32[]{:S(2)}) async-start(bf16[4,2,20480]{2,1,0:T(2,128)(2,1)} %reshape.136), calls=%async_computation | async-start | bytes 655360 | tf_op jit(solution)/shard_map/all_to_all | solution.py:73
  22.9 0.1 copy.67
  23.1 0.1 copy.69
  23.2 10.1 %all-to-all-done = bf16[4,2,20480]{2,1,0:T(2,128)(2,1)} async-done(((bf16[4,2,20480]{2,1,0:T(2,128)(2,1)}), bf16[4,2,20480]{2,1,0:T(2,128)(2,1)}, u32[]{:S(2)}, u32[]{:S(2)}) %all-to-all-start) | async-done | bytes 327712 | tf_op jit(solution)/shard_map/all_to_all | solution.py:73
  33.3 1.2 reshape.137
  34.6 0.7 fusion.23
  35.3 2.0 %multiply_add_fusion.1 = (f32[4,160,256]{2,0,1:T(4,128)S(1)}, f32[4,160,256]{2,0,1:T(4,128)}) fusion(f32[4,160,256]{2,0,1:T(4,128)S(1)} %fusion.23, f32[4,160]{0,1:T(8,128)S(1)} %copy.69, f32[4,160]{0,1:T(8,128)S(1)} %copy.67, bf16[4,160,256]{2,1,0:T(8,128)(2,1)S(1)} %bitcast.65), kind=kOutput, calls=%fused_computation.22 | convolution fusion | flops 9011424 | bytes 2298880 | tf_op jit(solution)/shard_map/kr,rmc->kmc/dot_general | solution.py:26
  37.3 1.0 copy.70
  38.3 3.5 %all-to-all-start.1 = ((f32[4,160,256]{2,1,0:T(8,128)}), f32[4,160,256]{2,1,0:T(8,128)S(1)}, u32[]{:S(2)}, u32[]{:S(2)}) async-start(f32[4,160,256]{2,1,0:T(8,128)} %copy.70), calls=%async_computation.1 | async-start | bytes 1310720 | tf_op jit(solution)/shard_map/all_to_all | solution.py:81
  41.8 2.1 %copy.72 = f32[4,160,256]{2,1,0:T(8,128)} copy(f32[4,160,256]{2,0,1:T(4,128)} %get-tuple-element.6) | data formatting | bytes 1310720 | tf_op jit(solution)/shard_map/sub | solution.py:79
  43.9 13.6 %all-to-all-done.1 = f32[4,160,256]{2,1,0:T(8,128)S(1)} async-done(((f32[4,160,256]{2,1,0:T(8,128)}), f32[4,160,256]{2,1,0:T(8,128)S(1)}, u32[]{:S(2)}, u32[]{:S(2)}) %all-to-all-start.1) | async-done | bytes 655392 | tf_op jit(solution)/shard_map/all_to_all | solution.py:81
  57.4 0.8 copy-done.1
  58.3 3.5 %all-to-all-start.2 = ((f32[4,160,256]{2,1,0:T(8,128)}), f32[4,160,256]{2,1,0:T(8,128)S(1)}, u32[]{:S(2)}, u32[]{:S(2)}) async-start(f32[4,160,256]{2,1,0:T(8,128)} %copy.72), calls=%async_computation.2 | async-start | bytes 1310720 | tf_op jit(solution)/shard_map/all_to_all | solution.py:82
  61.8 0.2 all-gather.2.cloned.1.call-start
  62.1 0.1 copy.77
  62.2 0.1 copy.74
  62.3 2.9 %fusion.20 = f32[8,80,256]{2,0,1:T(8,128)} fusion(f32[8,80,256]{2,1,0:T(8,128)} %bitcast.59), kind=kOutput, calls=%fused_computation.33 | convolution fusion | flops 15729536 | bytes 1310720 | tf_op jit(solution)/shard_map/kr,rmc->kmc/dot_general | solution.py:26
  65.2 13.1 %all-to-all-done.2 = f32[4,160,256]{2,1,0:T(8,128)S(1)} async-done(((f32[4,160,256]{2,1,0:T(8,128)}), f32[4,160,256]{2,1,0:T(8,128)S(1)}, u32[]{:S(2)}, u32[]{:S(2)}) %all-to-all-start.2) | async-done | bytes 655392 | tf_op jit(solution)/shard_map/all_to_all | solution.py:82
  78.3 1.0 fusion.16
  79.3 0.1 copy-done.2
  79.4 1.0 convolution_subtract_fusion.1
  80.5 1.2 multiply_subtract_fusion
  81.7 1.0 fusion.10
  82.7 1.0 fusion.14
  83.6 1.8 %convolution_subtract_fusion = f32[80,8,256]{2,0,1:T(8,128)} fusion(f32[80,8,256]{2,0,1:T(8,128)S(1)} %fusion.10, f32[8,80,256]{2,0,1:T(8,128)S(1)} %get-tuple-element.8), kind=kOutput, calls=%fused_computation.7 | convolution fusion | flops 157507840 | bytes 1966080 | tf_op jit(solution)/shard_map/qb,kbc->qkc/dot_general | solution.py:52
  85.5 1.0 convolution_add_fusion.1
  86.4 0.4 copy.80
  86.8 1.2 reshape_reshape.14
  88.0 2.1 %fusion.8 = f32[640,2,128]{0,2,1:T(8,128)S(1)} fusion(f32[640,2,128]{2,1,0:T(2,128)} %reshape_reshape.14), kind=kOutput, calls=%fused_computation.17 | convolution fusion | flops 251887616 | bytes 1310720 | tf_op jit(solution)/shard_map/ngc,cj->ngj/dot_general | solution.py:21
  90.1 1.2 copy.84
  91.4 2.3 %reshape_reshape.15 = f32[640,2,128]{2,1,0:T(2,128)} reshape(f32[80,8,256]{2,1,0:T(8,128)} %copy.84) | data formatting | bytes 1310720 | tf_op jit(solution)/shard_map/reshape;reshape | solution.py:20
  93.6 2.8 %fusion.5 = bf16[640,2,128]{0,2,1:T(8,128)(2,1)} fusion(f32[640,2,128]{0,2,1:T(8,128)S(1)} %fusion.8, f32[640,2,128]{2,1,0:T(2,128)} %reshape_reshape.15), kind=kOutput, calls=%fused_computation.13 | convolution fusion | flops 252379136 | bytes 1638400 | tf_op jit(solution)/shard_map/ngc,cj->ngj/dot_general | solution.py:21
  96.4 1.8 %reduce.1 = bf16[640,256]{0,1:T(8,128)(2,1)S(1)} reduce(bf16[640,1,256]{0,2,1:T(8,128)(2,1)} %bitcast.66, bf16[]{:T(256)} %broadcast.193), dimensions={1}, to_apply=%copy.86.reduce_sub_computation | reduce | bytes 655362 | tf_op jit(solution)/shard_map/convert_element_type | solution.py:88
  98.2 0.2 copy.120
  98.3 0.3 reshape.138
  98.6 12.9 %all_to_all.45 = bf16[4,2,20480]{2,1,0:T(2,128)(2,1)} all-to-all(bf16[4,2,20480]{2,1,0:T(2,128)(2,1)S(1)} %reshape.138), channel_id=1, replica_groups=mesh['grp'=2,'row'=4,'col'=4] {'row'}, dimensions={0} | all-to-all | bytes 655360 | tf_op jit(solution)/shard_map/all_to_all | solution.py:89
  111.6 1.2 reshape.139
  112.9 0.3 copy.87
  113.1 0.8 reshape.127
  114.0 4.3 %fusion.2 = f32[640,512]{1,0:T(8,128)} fusion(bf16[640,2048]{1,0:T(8,128)(2,1)S(1)} %copy-done, bf16[2048,512]{1,0:T(8,128)(2,1)} %param.6), kind=kOutput, calls=%fused_computation.4 | convolution fusion | flops 1343160320 | bytes 6029312 | tf_op jit(solution)/shard_map/dot_general | solution.py:96
  118.3 13.2 %all-gather.2.cloned.1.call-done = bf16[640,1024]{1,0:T(8,128)(2,1)} async-done(((bf16[640,256]{1,0:T(8,128)(2,1)}), bf16[640,1024]{1,0:T(8,128)(2,1)}) %all-gather.2.cloned.1.call-update) | async-done | bytes 1310736 | tf_op jit(solution)/shard_map/all_gather | solution.py:92
  131.5 3.7 %fusion.3 = bf16[640,512]{1,0:T(8,128)(2,1)} fusion(f32[640,512]{1,0:T(8,128)} %fusion.2, bf16[640,1024]{1,0:T(8,128)(2,1)} %all-gather.2.cloned.1.call-done, bf16[1024,512]{1,0:T(8,128)(2,1)} %param.7), kind=kOutput, calls=%fused_computation.5 | convolution fusion | flops 671744000 | bytes 4325376 | tf_op jit(solution)/shard_map/dot_general | solution.py:91
  (14 shorter events, 0.4 us)
Async XLA Ops:
  6.5 1.7 %copy-start = (bf16[640,2048]{1,0:T(8,128)(2,1)S(1)}, bf16[640,2048]{1,0:T(8,128)(2,1)}, u32[]{:S(2)}) copy-start(bf16[640,2048]{1,0:T(8,128)(2,1)} %param.4) | copy-start | bytes 7864324
  16.5 16.8 %all-to-all-start = ((bf16[4,2,20480]{2,1,0:T(2,128)(2,1)}), bf16[4,2,20480]{2,1,0:T(2,128)(2,1)}, u32[]{:S(2)}, u32[]{:S(2)}) async-start(bf16[4,2,20480]{2,1,0:T(2,128)(2,1)} %reshape.136), calls=%async_computation | async-start | bytes 655360 | tf_op jit(solution)/shard_map/all_to_all | solution.py:73
  38.3 19.1 %all-to-all-start.1 = ((f32[4,160,256]{2,1,0:T(8,128)}), f32[4,160,256]{2,1,0:T(8,128)S(1)}, u32[]{:S(2)}, u32[]{:S(2)}) async-start(f32[4,160,256]{2,1,0:T(8,128)} %copy.70), calls=%async_computation.1 | async-start | bytes 1310720 | tf_op jit(solution)/shard_map/all_to_all | solution.py:81
  57.4 0.8 copy-start.1
  58.3 20.0 %all-to-all-start.2 = ((f32[4,160,256]{2,1,0:T(8,128)}), f32[4,160,256]{2,1,0:T(8,128)S(1)}, u32[]{:S(2)}, u32[]{:S(2)}) async-start(f32[4,160,256]{2,1,0:T(8,128)} %copy.72), calls=%async_computation.2 | async-start | bytes 1310720 | tf_op jit(solution)/shard_map/all_to_all | solution.py:82
  61.8 69.8 %all-gather.2.cloned.1.call-start = ((), (), s32[]{:S(2)}) async-start(), calls=%async_computation.4 | async-start | bytes 1638400 | tf_op jit(solution)/shard_map/all_gather | solution.py:92
  78.3 1.1 copy-start.2
  79.4 1.1 copy-start.3
  88.0 2.1 %copy-start.4 = (f32[80,8,256]{2,0,1:T(8,128)S(1)}, f32[80,8,256]{2,0,1:T(8,128)}, u32[]{:S(2)}) copy-start(f32[80,8,256]{2,0,1:T(8,128)} %convolution_subtract_fusion) | copy-start | bytes 1966084
Sparse Core Ops, SparseCore 0:
  114.1 17.4 all-gather.1
where the time goes:
time: 143 us; the launch traced here: 142 us
  waiting for transfers between devices  50 us (35%)
  matrix products  28.6 us (20%)
  local copies, waits for them, and re-layouts  18.2 us (13%)
  between operations  13.6 us (10%)
  starting transfers between devices  13.5 us (9%)
  blocking collectives  12.9 us (9%)
  other arithmetic  5.24 us (4%)
    all_to_all x1, waiting for transfers between devices, on_device(): lax.all_to_all(turned_re, 'row', split_axis=0, concat_axis=1, tiled=True)  13.6 us
    all_gather x1, waiting for transfers between devices, on_device(): lax.all_gather(ordered, 'col', axis=1, tiled=True)  13.2 us
    all_to_all x1, waiting for transfers between devices, on_device(): lax.all_to_all(turned_im, 'row', split_axis=0, concat_axis=1, tiled=True)  13.1 us
    all_to_all x1, blocking collectives, on_device(): lax.all_to_all(scaled[:, None], 'row', split_axis=0, concat_axis=1, tiled...  12.9 us
    all_to_all x1, waiting for transfers between devices, on_device(): lax.all_to_all(lifted[None].astype(jnp.bfloat16), 'row', split_axis=1, co...  10.1 us
    dot_general x6, matrix products, across_rows(): jnp.einsum('kr,rmc->kmc', matrix, values, precision=lax.Precision.HIGHEST)  8.85 us
    unnamed x18, local copies, waits for them, and re-layouts  8.15 us
    all_to_all x1, starting transfers between devices, on_device(): lax.all_to_all(lifted[None].astype(jnp.bfloat16), 'row', split_axis=1, co...  6.35 us
  transfers between devices with their start and end apart: 4, of which 4 were waited for; matrix products, arithmetic and copies ran while one was open for 7% of the time, Pallas kernels for 0%

commit v1 on v0

--- a/solution.py
+++ b/solution.py
@@ -1,8 +1,12 @@
+import functools
 import math
 
 import jax
 import jax.numpy as jnp
+import numpy as np
 from jax import lax
+from jax.experimental import pallas as pl
+from jax.experimental.pallas import tpu as pltpu
 from jax.sharding import PartitionSpec as P
 
 GROUP_DIM = 128
@@ -97,9 +101,275 @@
     return (gate * proj).astype(jnp.bfloat16)
 
 
+MESH = pl.DeviceIdType.MESH
+TILE = 128
+
+
+def position_table(length, row_count):
+    place = np.arange(length)
+    order = place.reshape(-1, row_count).T.reshape(-1)
+    angle = 2.0 * np.pi * (np.outer(order, place) % (length * row_count)) / (length * row_count)
+    table = np.concatenate([np.cos(angle), np.sin(angle)], axis=1)
+    return table.reshape(row_count, length // row_count, 2 * length).astype(jnp.bfloat16)
+
+
+def group_table():
+    step = np.arange(GROUP_DIM)
+    angle = 2.0 * np.pi * (np.outer(step, step) % GROUP_DIM) / GROUP_DIM
+    return np.concatenate([np.cos(angle), np.sin(angle)], axis=1).astype(jnp.bfloat16)
+
+
+def dot32(a, b):
+    return jnp.dot(a, b, preferred_element_type=jnp.float32)
+
+
+def mixing_kernel(
+    tokens_hbm, four_hbm, gate_hbm, back_hbm, table_hbm, group_hbm, out_ref,
+    tokens, w_four, w_gate, w_back, table, group, turned, lines, spect, final, blocks, outer, gate, total,
+    load_sem, token_sem, line_send, line_recv, outer_send, outer_recv, col_send, col_recv,
+):
+    row, col = lax.axis_index("row"), lax.axis_index("col")
+    length = tokens.shape[0]
+    quarter = length // 4
+    tiles = length // TILE
+    groups = lines.shape[0]
+    scale = 1.0 / math.sqrt(4 * length * GROUP_DIM)
+    inner = jnp.logical_or(row == 1, row == 2)
+    sibling = col + 1 - 2 * (col % 2)
+    across = col + 2 - 4 * (col // 2)
+
+    loads = []
+    for at, (source, target) in enumerate(
+        ((four_hbm, w_four), (gate_hbm, w_gate), (table_hbm, table), (group_hbm, group), (back_hbm, w_back))
+    ):
+        loads.append(pltpu.make_async_copy(source, target, load_sem.at[at]))
+
+    def token_copy(tile):
+        rows = pl.ds(pl.multiple_of(tile * TILE, TILE), TILE)
+        return pltpu.make_async_copy(tokens_hbm.at[rows, :], tokens.at[rows, :], token_sem.at[tile])
+
+    loads[0].start()
+    for tile in range(tiles):
+        token_copy(tile).start()
+    for load in loads[1:]:
+        load.start()
+
+    barrier = pltpu.get_barrier_semaphore()
+    for step in (1, 2, 3):
+        pl.semaphore_signal(barrier, inc=1, device_id={"row": (row + step) % 4}, device_id_type=MESH)
+    for peer in (sibling, across):
+        pl.semaphore_signal(barrier, inc=1, device_id={"col": peer}, device_id_type=MESH)
+
+    loads[0].wait()
+
+    @pl.loop(0, tiles)
+    def _(tile):
+        token_copy(tile).wait()
+        rows = pl.ds(pl.multiple_of(tile * TILE, TILE), TILE)
+        feats = dot32(tokens[rows, :], w_four[...]).astype(jnp.bfloat16)
+        for g in range(groups):
+            lines[g, row, rows, :] = feats[:, g * GROUP_DIM : (g + 1) * GROUP_DIM]
+
+    pl.semaphore_wait(barrier, 5)
+
+    def line_copy(g, origin, target, at):
+        return pltpu.make_async_remote_copy(
+            src_ref=lines.at[g, origin],
+            dst_ref=lines.at[g, origin],
+            send_sem=line_send.at[g, at],
+            recv_sem=line_recv.at[g, origin],
+            device_id={"row": target},
+            device_id_type=MESH,
+        )
+
+    for g in range(groups):
+
+        @pl.when(inner)
+        def _():
+            line_copy(g, row, 3 - row, 0).start()
+
+        @pl.when(jnp.logical_not(inner))
+        def _():
+            near = 1 + row // 3
+            line_copy(g, row, 3 - near, 0).start()
+            line_copy(g, row, near, 1).start()
+
+    loads[1].wait()
+
+    @pl.loop(0, tiles)
+    def _(tile):
+        rows = pl.ds(pl.multiple_of(tile * TILE, TILE), TILE)
+        gate[rows, :] = jax.nn.sigmoid(dot32(tokens[rows, :], w_gate[...]))
+
+    for load in loads[2:]:
+        load.wait()
+
+    @pl.when(inner)
+    def _():
+        for at, out_row in enumerate((3 * (row - 1), row)):
+            turn = out_row * lax.broadcasted_iota(jnp.int32, (quarter, length), 1) % 4
+            for s in range(4):
+                cos_at = table[s, :, :length].astype(jnp.float32)
+                sin_at = table[s, :, length:].astype(jnp.float32)
+                odd, minus = turn % 2 == 1, jnp.where(turn >= 2, -1.0, 1.0)
+                turned_cos = jnp.where(odd, -sin_at, cos_at) * minus
+                turned_sin = jnp.where(odd, cos_at, sin_at) * minus
+                turned[at, s, :, :length] = turned_cos.astype(jnp.bfloat16)
+                turned[at, s, :, length:] = (-turned_sin).astype(jnp.bfloat16)
+
+    def outer_copy(g):
+        return pltpu.make_async_remote_copy(
+            src_ref=outer.at[g],
+            dst_ref=blocks.at[g, 0],
+            send_sem=outer_send.at[g],
+            recv_sem=outer_recv.at[g],
+            device_id={"row": 3 * (row // 2)},
+            device_id_type=MESH,
+        )
+
+    def col_copy(g, source, slot, target):
+        return pltpu.make_async_remote_copy(
+            src_ref=blocks.at[g, source],
+            dst_ref=blocks.at[g, slot],
+            send_sem=col_send.at[g, slot],
+            recv_sem=col_recv.at[g, slot],
+            device_id={"col": target},
+            device_id_type=MESH,
+        )
+
+    def transform(g):
+        for step in (1, 2, 3):
+            origin = (row + step) % 4
+            pltpu.make_async_copy(lines.at[g, origin], lines.at[g, origin], line_recv.at[g, origin]).wait()
+
+        @pl.loop(0, tiles)
+        def _(tile):
+            start = pl.multiple_of(tile * TILE, TILE)
+            rows, low = pl.ds(start, TILE), pl.ds(pl.multiple_of(length + start, TILE), TILE)
+            x0, x1, x2, x3 = (lines[g, at, rows, :].astype(jnp.float32) for at in range(4))
+            even, odd = x0 + x2, x1 + x3
+            parts = (even + odd, x0 - x2, even - odd, x1 - x3)
+            mixed = [dot32(part.astype(jnp.bfloat16), group[...]) for part in parts]
+            cos_of = [part[:, :GROUP_DIM] for part in mixed]
+            sin_of = [part[:, GROUP_DIM:] for part in mixed]
+            for s in (0, 2):
+                spect[s, rows, :] = cos_of[s].astype(jnp.bfloat16)
+                spect[s, low, :] = sin_of[s].astype(jnp.bfloat16)
+            spect[1, rows, :] = (cos_of[1] - sin_of[3]).astype(jnp.bfloat16)
+            spect[1, low, :] = (sin_of[1] + cos_of[3]).astype(jnp.bfloat16)
+            spect[3, rows, :] = (cos_of[1] + sin_of[3]).astype(jnp.bfloat16)
+            spect[3, low, :] = (sin_of[1] - cos_of[3]).astype(jnp.bfloat16)
+
+        for at in range(2):
+            for s in range(4):
+                final[at, pl.ds(s, quarter, stride=4), :] = dot32(turned[at, s], spect[s]) * scale
+            if at == 0:
+                outer[g] = final[at].astype(jnp.bfloat16)
+                outer_copy(g).start()
+            else:
+                blocks[g, 0] = final[at].astype(jnp.bfloat16)
+
+    def back_rows(g, peer):
+        return w_back[pl.ds(pl.multiple_of((peer * groups + g) * GROUP_DIM, GROUP_DIM), GROUP_DIM), :]
+
+    opposite = across + 1 - 2 * (across % 2)
+    for g in range(groups):
+        pl.when(inner)(functools.partial(transform, g))
+
+        @pl.when(jnp.logical_not(inner))
+        def _():
+            outer_copy(g).wait_recv()
+
+        col_copy(g, 0, 2, across).start()
+        col_copy(g, 0, 1, sibling).start()
+        col_copy(g, 0, 1, sibling).wait_recv()
+
+        @pl.loop(0, tiles)
+        def _(tile):
+            rows = pl.ds(pl.multiple_of(tile * TILE, TILE), TILE)
+            share = dot32(blocks[g, 0, rows, :], back_rows(g, col)) + dot32(
+                blocks[g, 1, rows, :], back_rows(g, sibling)
+            )
+            total[rows, :] = share if g == 0 else total[rows, :] + share
+
+        col_copy(g, 0, 2, across).wait_recv()
+        col_copy(g, 2, 3, sibling).start()
+        col_copy(g, 2, 3, sibling).wait_recv()
+
+        @pl.loop(0, tiles)
+        def _(tile):
+            rows = pl.ds(pl.multiple_of(tile * TILE, TILE), TILE)
+            share = dot32(blocks[g, 2, rows, :], back_rows(g, across)) + dot32(
+                blocks[g, 3, rows, :], back_rows(g, opposite)
+            )
+            summed = total[rows, :] + share
+            if g < groups - 1:
+                total[rows, :] = summed
+            else:
+                out_ref[rows, :] = (gate[rows, :] * summed).astype(jnp.bfloat16)
+
+    for g in range(groups):
+        for slot in (1, 2, 3):
+            col_copy(g, 0 if slot < 3 else 2, slot, sibling).wait_send()
+        line_copy(g, row, 3 - row, 0).wait_send()
+
+        @pl.when(inner)
+        def _():
+            outer_copy(g).wait_send()
+
+        @pl.when(jnp.logical_not(inner))
+        def _():
+            line_copy(g, row, 3 - row, 1).wait_send()
+
+
+def on_line(tokens, w_four, w_gate, w_back):
+    length, width = tokens.shape
+    groups = w_four.shape[1] // GROUP_DIM
+    features = w_gate.shape[1]
+    quarter = length // 4
+    low = jnp.bfloat16
+    table = jnp.asarray(position_table(length, 4))
+    group = jnp.asarray(group_table())
+    hbm = pl.BlockSpec(memory_space=pl.ANY)
+    return pl.pallas_call(
+        mixing_kernel,
+        out_shape=jax.ShapeDtypeStruct((length, features), low),
+        in_specs=[hbm] * 6,
+        out_specs=pl.BlockSpec(memory_space=pltpu.VMEM),
+        scratch_shapes=[
+            pltpu.VMEM(tokens.shape, low),
+            pltpu.VMEM(w_four.shape, low),
+            pltpu.VMEM(w_gate.shape, low),
+            pltpu.VMEM(w_back.shape, low),
+            pltpu.VMEM(table.shape, low),
+            pltpu.VMEM(group.shape, low),
+            pltpu.VMEM((2,) + table.shape, low),
+            pltpu.VMEM((groups, 4, length, GROUP_DIM), low),
+            pltpu.VMEM((4, 2 * length, GROUP_DIM), low),
+            pltpu.VMEM((2, length, GROUP_DIM), jnp.float32),
+            pltpu.VMEM((groups, 4, length, GROUP_DIM), low),
+            pltpu.VMEM((groups, length, GROUP_DIM), low),
+            pltpu.VMEM((length, features), jnp.float32),
+            pltpu.VMEM((length, features), jnp.float32),
+            pltpu.SemaphoreType.DMA((5,)),
+            pltpu.SemaphoreType.DMA((length // TILE,)),
+            pltpu.SemaphoreType.DMA((groups, 2)),
+            pltpu.SemaphoreType.DMA((groups, 4)),
+            pltpu.SemaphoreType.DMA((groups,)),
+            pltpu.SemaphoreType.DMA((groups,)),
+            pltpu.SemaphoreType.DMA((groups, 4)),
+            pltpu.SemaphoreType.DMA((groups, 4)),
+        ],
+        compiler_params=pltpu.CompilerParams(
+            collective_id=0, has_side_effects=True, vmem_limit_bytes=60 * 1024 * 1024
+        ),
+    )(tokens, w_four, w_gate, w_back, table, group)
+
+
 def solution(mesh):
+    square = mesh.shape["row"] == 4 and mesh.shape["col"] == 4
     return jax.shard_map(
-        on_device,
+        on_line if square else on_device,
         mesh=mesh,
         in_specs=(P(("grp", "row"), None), P(None, "col"), P(None, "col"), P(None, "col")),
         out_specs=P(("grp", "row"), "col"),

time: 143 us -> 42.4 us (0.30)
  waiting for transfers between devices: 50 us -> 0 us
  Pallas kernels: 0 us -> 40.2 us
  matrix products: 28.6 us -> 0 us
  local copies, waits for them, and re-layouts: 18.2 us -> 1.97 us
  between operations: 13.6 us -> 0.01 us
  starting transfers between devices: 13.5 us -> 0 us
  blocking collectives: 12.9 us -> 0 us
  other arithmetic: 5.24 us -> 0 us
    pallas_call x0 -> x1, Pallas kernels: none -> 40.2 us  [on_line(): pl.pallas_call(mixing_kernel, out_shape=jax.ShapeDtypeStruct((length, fea...]
    all_to_all x3 -> x0, waiting for transfers between devices: 36.8 us -> none  [the longest x1 13.6 us: on_device(): lax.all_to_all(turned_re, 'row', split_axis=0, concat_axis=1, tiled=True)]
    dot_general x15 -> x0, matrix products: 28.6 us -> none  [the longest x6 8.85 us: across_rows(): jnp.einsum('kr,rmc->kmc', matrix, values, precision=lax.Precision.HIGHEST)]
    all_to_all x3 -> x0, starting transfers between devices: 13.3 us -> none  [the longest x1 6.35 us: on_device(): lax.all_to_all(lifted[None].astype(jnp.bfloat16), 'row', split_axis=1, co...]
    all_gather x1 -> x0, waiting for transfers between devices: 13.2 us -> none  [on_device(): lax.all_gather(ordered, 'col', axis=1, tiled=True)]
    all_to_all x1 -> x0, blocking collectives: 12.9 us -> none  [on_device(): lax.all_to_all(scaled[:, None], 'row', split_axis=0, concat_axis=1, tiled...]
    unnamed x18 -> x1, local copies, waits for them, and re-layouts: 8.15 us -> 1.97 us
    another operation x2 -> x0, local copies, waits for them, and re-layouts: 3.41 us -> none  [channel_mix(): shaped = values.reshape(height, -1, GROUP_DIM)]
  transfers between devices with their start and end apart: 4 -> 0, of which waited for: 4 -> 0; matrix products, arithmetic and copies ran while one was open for 7% -> 0% of each run, Pallas kernels for 0% -> 0%
where the time goes in v1:
time: 42.4 us; the launch traced here: 42.2 us
  Pallas kernels  40.2 us (95%)
  local copies, waits for them, and re-layouts  1.97 us (5%)
    pallas_call x1, Pallas kernels, on_line(): pl.pallas_call(mixing_kernel, out_shape=jax.ShapeDtypeStruct((length, fea...  40.2 us
    unnamed x1, local copies, waits for them, and re-layouts  1.97 us

profile of v1, /device:TPU:0, one launch (start us, length us, event | category | flops | bytes accessed | tf_op | source)
XLA Modules:
  0.0 42.2 jit_solution(9717372237114245931)
XLA Ops:
  0.0 40.2 %shard_map.64 = bf16[640,512]{1,0:T(8,128)(2,1)} custom-call(bf16[640,2048]{1,0:T(8,128)(2,1)} %tokens_hbm.1, bf16[2048,256]{1,0:T(8,128)(2,1)} %four_hbm.1, bf16[2048,512]{1,0:T(8,128)(2,1)} %gate_hbm.1, bf16[1024,512]{1,0:T(8,128)(2,1)} %back_hbm.1, bf16[4,160,1280]{2,1,0:T(8,128)(2,1)} %constant.4.clone.table_hbm, bf16[128,256]{1,0:T(8,128)(2,1)} %constant.5.clone.group_hbm), custom_call_target="tpu_custom_call" | custom-call | tf_op jit(solution)/shard_map/pallas_call | solution.py:334
  40.2 2.0 %copy.8 = bf16[640,512]{1,0:T(8,128)(2,1)} copy(bf16[640,512]{1,0:T(8,128)(2,1)} %shard_map.64) | data formatting | bytes 1310720

commit v2 on v0

--- a/solution.py
+++ b/solution.py
@@ -1,8 +1,12 @@
+import functools
 import math
 
 import jax
 import jax.numpy as jnp
+import numpy as np
 from jax import lax
+from jax.experimental import pallas as pl
+from jax.experimental.pallas import tpu as pltpu
 from jax.sharding import PartitionSpec as P
 
 GROUP_DIM = 128
@@ -97,9 +101,317 @@
     return (gate * proj).astype(jnp.bfloat16)
 
 
+MESH = pl.DeviceIdType.MESH
+TILE = 160
+
+
+def position_table(length, row_count):
+    place = np.arange(length)
+    order = place.reshape(-1, row_count).T.reshape(-1)
+    angle = 2.0 * np.pi * (np.outer(order, place) % (length * row_count)) / (length * row_count)
+    table = np.concatenate([np.cos(angle), np.sin(angle)], axis=1)
+    return table.reshape(row_count, length // row_count, 2 * length).astype(jnp.bfloat16)
+
+
+def group_table():
+    step = np.arange(GROUP_DIM)
+    angle = 2.0 * np.pi * (np.outer(step, step) % GROUP_DIM) / GROUP_DIM
+    return np.concatenate([np.cos(angle), np.sin(angle)], axis=1).astype(jnp.bfloat16)
+
+
+def dot32(a, b):
+    return jnp.dot(a, b, preferred_element_type=jnp.float32)
+
+
+def mixing_kernel(
+    tokens_hbm, four_hbm, gate_hbm, back_hbm, table_hbm, group_hbm, out_hbm,
+    tokens, w_four, w_gate, w_back, table, group, turned, lines, spect, final, blocks, outer, gate, total, ready,
+    load_sem, token_sem, line_send, line_recv, outer_send, outer_recv, col_send, col_recv, out_sem,
+):
+    row, col = lax.axis_index("row"), lax.axis_index("col")
+    length = tokens.shape[0]
+    quarter, half = length // 4, length // 2
+    tiles = length // TILE
+    groups = lines.shape[0]
+    scale = 1.0 / math.sqrt(4 * length * GROUP_DIM)
+    inner = jnp.logical_or(row == 1, row == 2)
+    ends = jnp.logical_not(inner)
+    end_row = 3 * (row // 2)
+    sibling = col + 1 - 2 * (col % 2)
+    across = col + 2 - 4 * (col // 2)
+    opposite = across + 1 - 2 * (across % 2)
+
+    loads = []
+    for at, (source, target) in enumerate(
+        ((four_hbm, w_four), (gate_hbm, w_gate), (table_hbm, table), (group_hbm, group), (back_hbm, w_back))
+    ):
+        loads.append(pltpu.make_async_copy(source, target, load_sem.at[at]))
+
+    def tile_rows(tile):
+        return pl.ds(pl.multiple_of(tile * TILE, TILE), TILE)
+
+    def token_copy(tile):
+        return pltpu.make_async_copy(tokens_hbm.at[tile_rows(tile), :], tokens.at[tile_rows(tile), :], token_sem.at[tile])
+
+    loads[0].start()
+    for tile in range(tiles):
+        token_copy(tile).start()
+    for load in loads[1:]:
+        load.start()
+
+    barrier = pltpu.get_barrier_semaphore()
+    for step in (1, 2, 3):
+        pl.semaphore_signal(barrier, inc=1, device_id={"row": (row + step) % 4}, device_id_type=MESH)
+    for peer in (sibling, across):
+        pl.semaphore_signal(barrier, inc=1, device_id={"col": peer}, device_id_type=MESH)
+
+    def line_copy(g, part, origin, target, at):
+        rows = pl.ds(part * half, half)
+        return pltpu.make_async_remote_copy(
+            src_ref=lines.at[g, origin, rows],
+            dst_ref=lines.at[g, origin, rows],
+            send_sem=line_send.at[at, g, part],
+            recv_sem=line_recv.at[g, part, origin],
+            device_id={"row": target},
+            device_id_type=MESH,
+        )
+
+    near = 1 + row // 2
+    own_target = jnp.where(inner, 3 - row, near)
+
+    def feats(tile):
+        values = dot32(tokens[tile_rows(tile), :], w_four[...]).astype(jnp.bfloat16)
+        for g in range(groups):
+            lines[g, row, tile_rows(tile), :] = values[:, g * GROUP_DIM : (g + 1) * GROUP_DIM]
+
+    loads[0].wait()
+    for part in range(2):
+
+        @pl.loop(part * tiles // 2, (part + 1) * tiles // 2)
+        def _(tile):
+            token_copy(tile).wait()
+            feats(tile)
+
+        if part == 0:
+            pl.semaphore_wait(barrier, 5)
+        line_copy(0, part, row, own_target, 0).start()
+    for g in range(1, groups):
+        for part in range(2):
+            line_copy(g, part, row, own_target, 0).start()
+
+    loads[1].wait()
+
+    @pl.loop(0, tiles)
+    def _(tile):
+        gate[tile_rows(tile), :] = jax.nn.sigmoid(dot32(tokens[tile_rows(tile), :], w_gate[...]))
+
+    for load in loads[2:]:
+        load.wait()
+
+    def relay(g):
+        for part in range(2):
+            line_copy(g, part, end_row, 3 - row, 1).wait_recv()
+            line_copy(g, part, end_row, 3 - row, 1).start()
+
+    def turn_tables():
+        for at, out_row in enumerate((end_row, row)):
+            turn = out_row * lax.broadcasted_iota(jnp.int32, (quarter, length), 1) % 4
+            odd, minus = turn % 2 == 1, jnp.where(turn >= 2, -1.0, 1.0)
+            for s in range(4):
+                cos_at = table[s, :, :length].astype(jnp.float32)
+                sin_at = table[s, :, length:].astype(jnp.float32)
+                turned_cos = jnp.where(odd, -sin_at, cos_at) * minus
+                turned_sin = jnp.where(odd, cos_at, sin_at) * minus
+                turned[at, s, :, :length] = turned_cos.astype(jnp.bfloat16)
+                turned[at, s, :, length:] = (-turned_sin).astype(jnp.bfloat16)
+
+    @pl.when(inner)
+    def _():
+        relay(0)
+        turn_tables()
+        for g in range(1, groups):
+            relay(g)
+
+    def outer_copy(g, part):
+        rows = pl.ds(part * half, half)
+        return pltpu.make_async_remote_copy(
+            src_ref=outer.at[g, rows],
+            dst_ref=blocks.at[g, 0, rows],
+            send_sem=outer_send.at[g, part],
+            recv_sem=outer_recv.at[g, part],
+            device_id={"row": end_row},
+            device_id_type=MESH,
+        )
+
+    def col_copy(g, part, source, slot, target):
+        rows = pl.ds(part * half, half)
+        return pltpu.make_async_remote_copy(
+            src_ref=blocks.at[g, source, rows],
+            dst_ref=blocks.at[g, slot, rows],
+            send_sem=col_send.at[g, part, slot],
+            recv_sem=col_recv.at[g, part, slot],
+            device_id={"col": target},
+            device_id_type=MESH,
+        )
+
+    def share_own(g, part):
+        col_copy(g, part, 0, 2, across).start()
+        col_copy(g, part, 0, 1, sibling).start()
+
+    def transform(g):
+        for part in range(2):
+            for origin in (3 - row, 3 - end_row):
+                line_copy(g, part, origin, 3 - row, 0).wait_recv()
+
+            @pl.loop(part * tiles // 2, (part + 1) * tiles // 2)
+            def _(tile):
+                rows, low = tile_rows(tile), tile_rows(tiles + tile)
+                x0, x1, x2, x3 = (lines[g, at, rows, :].astype(jnp.float32) for at in range(4))
+                even, odd = x0 + x2, x1 + x3
+                parts = (even + odd, x0 - x2, even - odd, x1 - x3)
+                mixed = [dot32(value.astype(jnp.bfloat16), group[...]) for value in parts]
+                cos_of = [value[:, :GROUP_DIM] for value in mixed]
+                sin_of = [value[:, GROUP_DIM:] for value in mixed]
+                for s in (0, 2):
+                    spect[s, rows, :] = cos_of[s].astype(jnp.bfloat16)
+                    spect[s, low, :] = sin_of[s].astype(jnp.bfloat16)
+                spect[1, rows, :] = (cos_of[1] - sin_of[3]).astype(jnp.bfloat16)
+                spect[1, low, :] = (sin_of[1] + cos_of[3]).astype(jnp.bfloat16)
+                spect[3, rows, :] = (cos_of[1] + sin_of[3]).astype(jnp.bfloat16)
+                spect[3, low, :] = (sin_of[1] - cos_of[3]).astype(jnp.bfloat16)
+
+        for at in range(2):
+            for part in range(2):
+                rows = pl.ds(part * half, half)
+                some = pl.ds(part * quarter // 2, quarter // 2)
+                for s in range(4):
+                    value = dot32(turned[at, s, some, :], spect[s]) * scale
+                    final[at, pl.ds(part * half + s, quarter // 2, stride=4), :] = value
+                if at == 0:
+                    outer[g, rows, :] = final[at, rows, :].astype(jnp.bfloat16)
+                    outer_copy(g, part).start()
+                else:
+                    blocks[g, 0, rows, :] = final[at, rows, :].astype(jnp.bfloat16)
+                    share_own(g, part)
+
+    def receive(g):
+        for part in range(2):
+            outer_copy(g, part).wait_recv()
+            share_own(g, part)
+
+    def back_rows(g, peer):
+        return w_back[pl.ds(pl.multiple_of((peer * groups + g) * GROUP_DIM, GROUP_DIM), GROUP_DIM), :]
+
+    def out_copy(part):
+        rows = pl.ds(part * half, half)
+        return pltpu.make_async_copy(ready.at[rows, :], out_hbm.at[rows, :], out_sem.at[part])
+
+    def finish(g):
+        for part in range(2):
+            col_copy(g, part, 0, 1, sibling).wait_recv()
+
+            @pl.loop(part * tiles // 2, (part + 1) * tiles // 2)
+            def _(tile):
+                rows = tile_rows(tile)
+                share = dot32(blocks[g, 0, rows, :], back_rows(g, col))
+                share = share + dot32(blocks[g, 1, rows, :], back_rows(g, sibling))
+                total[rows, :] = share if g == 0 else total[rows, :] + share
+
+        for part in range(2):
+            col_copy(g, part, 0, 2, across).wait_recv()
+            col_copy(g, part, 2, 3, sibling).start()
+        for part in range(2):
+            col_copy(g, part, 2, 3, sibling).wait_recv()
+
+            @pl.loop(part * tiles // 2, (part + 1) * tiles // 2)
+            def _(tile):
+                rows = tile_rows(tile)
+                share = dot32(blocks[g, 2, rows, :], back_rows(g, across))
+                share = share + dot32(blocks[g, 3, rows, :], back_rows(g, opposite))
+                summed = total[rows, :] + share
+                if g < groups - 1:
+                    total[rows, :] = summed
+                else:
+                    ready[rows, :] = (gate[rows, :] * summed).astype(jnp.bfloat16)
+
+            if g == groups - 1:
+                out_copy(part).start()
+
+    @pl.when(inner)
+    def _():
+        for g in range(groups):
+            transform(g)
+
+    for g in range(groups):
+        pl.when(ends)(functools.partial(receive, g))
+        finish(g)
+
+    for part in range(2):
+        for g in range(groups):
+            for slot in (1, 2, 3):
+                col_copy(g, part, 0 if slot < 3 else 2, slot, sibling).wait_send()
+            line_copy(g, part, row, own_target, 0).wait_send()
+    for part in range(2):
+
+        @pl.when(inner)
+        def _():
+            for g in range(groups):
+                outer_copy(g, part).wait_send()
+                line_copy(g, part, end_row, 3 - row, 1).wait_send()
+
+        out_copy(part).wait()
+
+
+def on_line(tokens, w_four, w_gate, w_back):
+    length, width = tokens.shape
+    groups = w_four.shape[1] // GROUP_DIM
+    features = w_gate.shape[1]
+    quarter = length // 4
+    low = jnp.bfloat16
+    table = jnp.asarray(position_table(length, 4))
+    group = jnp.asarray(group_table())
+    hbm = pl.BlockSpec(memory_space=pl.ANY)
+    return pl.pallas_call(
+        mixing_kernel,
+        out_shape=jax.ShapeDtypeStruct((length, features), low),
+        in_specs=[hbm] * 6,
+        out_specs=hbm,
+        scratch_shapes=[
+            pltpu.VMEM(tokens.shape, low),
+            pltpu.VMEM(w_four.shape, low),
+            pltpu.VMEM(w_gate.shape, low),
+            pltpu.VMEM(w_back.shape, low),
+            pltpu.VMEM(table.shape, low),
+            pltpu.VMEM(group.shape, low),
+            pltpu.VMEM((2,) + table.shape, low),
+            pltpu.VMEM((groups, 4, length, GROUP_DIM), low),
+            pltpu.VMEM((4, 2 * length, GROUP_DIM), low),
+            pltpu.VMEM((2, length, GROUP_DIM), jnp.float32),
+            pltpu.VMEM((groups, 4, length, GROUP_DIM), low),
+            pltpu.VMEM((groups, length, GROUP_DIM), low),
+            pltpu.VMEM((length, features), jnp.float32),
+            pltpu.VMEM((length, features), jnp.float32),
+            pltpu.VMEM((length, features), low),
+            pltpu.SemaphoreType.DMA((5,)),
+            pltpu.SemaphoreType.DMA((length // TILE,)),
+            pltpu.SemaphoreType.DMA((2, groups, 2)),
+            pltpu.SemaphoreType.DMA((groups, 2, 4)),
+            pltpu.SemaphoreType.DMA((groups, 2)),
+            pltpu.SemaphoreType.DMA((groups, 2)),
+            pltpu.SemaphoreType.DMA((groups, 2, 4)),
+            pltpu.SemaphoreType.DMA((groups, 2, 4)),
+            pltpu.SemaphoreType.DMA((2,)),
+        ],
+        compiler_params=pltpu.CompilerParams(
+            collective_id=0, has_side_effects=True, vmem_limit_bytes=60 * 1024 * 1024
+        ),
+    )(tokens, w_four, w_gate, w_back, table, group)
+
+
 def solution(mesh):
+    square = mesh.shape["row"] == 4 and mesh.shape["col"] == 4
     return jax.shard_map(
-        on_device,
+        on_line if square else on_device,
         mesh=mesh,
         in_specs=(P(("grp", "row"), None), P(None, "col"), P(None, "col"), P(None, "col")),
         out_specs=P(("grp", "row"), "col"),

time: 143 us -> 38.8 us (0.27)
  waiting for transfers between devices: 50 us -> 0 us
  Pallas kernels: 0 us -> 36.7 us
  matrix products: 28.6 us -> 0 us
  local copies, waits for them, and re-layouts: 18.2 us -> 1.97 us
  between operations: 13.6 us -> 0.01 us
  starting transfers between devices: 13.5 us -> 0 us
  blocking collectives: 12.9 us -> 0 us
  other arithmetic: 5.24 us -> 0 us
    all_to_all x3 -> x0, waiting for transfers between devices: 36.8 us -> none  [the longest x1 13.6 us: on_device(): lax.all_to_all(turned_re, 'row', split_axis=0, concat_axis=1, tiled=True)]
    pallas_call x0 -> x1, Pallas kernels: none -> 36.7 us  [on_line(): pl.pallas_call(mixing_kernel, out_shape=jax.ShapeDtypeStruct((length, fea...]
    dot_general x15 -> x0, matrix products: 28.6 us -> none  [the longest x6 8.85 us: across_rows(): jnp.einsum('kr,rmc->kmc', matrix, values, precision=lax.Precision.HIGHEST)]
    all_to_all x3 -> x0, starting transfers between devices: 13.3 us -> none  [the longest x1 6.35 us: on_device(): lax.all_to_all(lifted[None].astype(jnp.bfloat16), 'row', split_axis=1, co...]
    all_gather x1 -> x0, waiting for transfers between devices: 13.2 us -> none  [on_device(): lax.all_gather(ordered, 'col', axis=1, tiled=True)]
    all_to_all x1 -> x0, blocking collectives: 12.9 us -> none  [on_device(): lax.all_to_all(scaled[:, None], 'row', split_axis=0, concat_axis=1, tiled...]
    unnamed x18 -> x1, local copies, waits for them, and re-layouts: 8.15 us -> 1.97 us
    another operation x2 -> x0, local copies, waits for them, and re-layouts: 3.41 us -> none  [channel_mix(): shaped = values.reshape(height, -1, GROUP_DIM)]
  transfers between devices with their start and end apart: 4 -> 0, of which waited for: 4 -> 0; matrix products, arithmetic and copies ran while one was open for 7% -> 0% of each run, Pallas kernels for 0% -> 0%
where the time goes in v2:
time: 38.8 us; the launch traced here: 38.7 us
  Pallas kernels  36.7 us (95%)
  local copies, waits for them, and re-layouts  1.97 us (5%)
    pallas_call x1, Pallas kernels, on_line(): pl.pallas_call(mixing_kernel, out_shape=jax.ShapeDtypeStruct((length, fea...  36.7 us
    unnamed x1, local copies, waits for them, and re-layouts  1.97 us

profile of v2, /device:TPU:0, one launch (start us, length us, event | category | flops | bytes accessed | tf_op | source)
XLA Modules:
  0.0 38.7 jit_solution(5239812182130192984)
XLA Ops:
  0.0 36.7 %shard_map.64 = bf16[640,512]{1,0:T(8,128)(2,1)} custom-call(bf16[640,2048]{1,0:T(8,128)(2,1)} %tokens_hbm.1, bf16[2048,256]{1,0:T(8,128)(2,1)} %four_hbm.1, bf16[2048,512]{1,0:T(8,128)(2,1)} %gate_hbm.1, bf16[1024,512]{1,0:T(8,128)(2,1)} %back_hbm.1, bf16[4,160,1280]{2,1,0:T(8,128)(2,1)} %constant.4.clone.table_hbm, bf16[128,256]{1,0:T(8,128)(2,1)} %constant.5.clone.group_hbm), custom_call_target="tpu_custom_call" | custom-call | tf_op jit(solution)/shard_map/pallas_call | solution.py:374
  36.7 2.0 %copy.8 = bf16[640,512]{1,0:T(8,128)(2,1)} copy(bf16[640,512]{1,0:T(8,128)(2,1)} %shard_map.64) | data formatting | bytes 1310720

commit v3 on v2

--- a/solution.py
+++ b/solution.py
@@ -156,9 +156,6 @@
     loads[0].start()
     for tile in range(tiles):
         token_copy(tile).start()
-    for load in loads[1:]:
-        load.start()
-
     barrier = pltpu.get_barrier_semaphore()
     for step in (1, 2, 3):
         pl.semaphore_signal(barrier, inc=1, device_id={"row": (row + step) % 4}, device_id_type=MESH)
@@ -195,9 +192,16 @@
         if part == 0:
             pl.semaphore_wait(barrier, 5)
         line_copy(0, part, row, own_target, 0).start()
+        if part == 0:
+            for load in loads[1:]:
+                load.start()
     for g in range(1, groups):
-        for part in range(2):
-            line_copy(g, part, row, own_target, 0).start()
+        line_copy(g, 0, row, own_target, 0).start()
+
+    @pl.when(ends)
+    def _():
+        for g in range(1, groups):
+            line_copy(g, 1, row, own_target, 0).start()
 
     loads[1].wait()
 
@@ -228,6 +232,8 @@
     @pl.when(inner)
     def _():
         relay(0)
+        for g in range(1, groups):
+            line_copy(g, 1, row, own_target, 0).start()
         turn_tables()
         for g in range(1, groups):
             relay(g)
@@ -320,15 +326,19 @@
         for part in range(2):
             col_copy(g, part, 0, 2, across).wait_recv()
             col_copy(g, part, 2, 3, sibling).start()
-        for part in range(2):
-            col_copy(g, part, 2, 3, sibling).wait_recv()
 
             @pl.loop(part * tiles // 2, (part + 1) * tiles // 2)
             def _(tile):
                 rows = tile_rows(tile)
-                share = dot32(blocks[g, 2, rows, :], back_rows(g, across))
-                share = share + dot32(blocks[g, 3, rows, :], back_rows(g, opposite))
-                summed = total[rows, :] + share
+                total[rows, :] += dot32(blocks[g, 2, rows, :], back_rows(g, across))
+
+        for part in range(2):
+            col_copy(g, part, 2, 3, sibling).wait_recv()
+
+            @pl.loop(part * tiles // 2, (part + 1) * tiles // 2)
+            def _(tile):
+                rows = tile_rows(tile)
+                summed = total[rows, :] + dot32(blocks[g, 3, rows, :], back_rows(g, opposite))
                 if g < groups - 1:
                     total[rows, :] = summed
                 else:
@@ -370,12 +380,13 @@
     low = jnp.bfloat16
     table = jnp.asarray(position_table(length, 4))
     group = jnp.asarray(group_table())
-    hbm = pl.BlockSpec(memory_space=pl.ANY)
+    tokens, w_four, w_gate, w_back, table, group = (pltpu.with_memory_space_constraint(x, pltpu.HBM) for x in (tokens, w_four, w_gate, w_back, table, group))
+    hbm = pl.BlockSpec(memory_space=pltpu.HBM)
     return pl.pallas_call(
         mixing_kernel,
         out_shape=jax.ShapeDtypeStruct((length, features), low),
         in_specs=[hbm] * 6,
-        out_specs=hbm,
+        out_specs=pl.BlockSpec(memory_space=pl.ANY),
         scratch_shapes=[
             pltpu.VMEM(tokens.shape, low),
             pltpu.VMEM(w_four.shape, low),
@@ -403,7 +414,7 @@
             pltpu.SemaphoreType.DMA((2,)),
         ],
         compiler_params=pltpu.CompilerParams(
-            collective_id=0, has_side_effects=True, vmem_limit_bytes=60 * 1024 * 1024
+            collective_id=0, has_side_effects=True, vmem_limit_bytes=28 * 1024 * 1024
         ),
     )(tokens, w_four, w_gate, w_back, table, group)
 

time: 38.8 us -> 35.1 us (0.905)
  Pallas kernels: 36.7 us -> 34.1 us
  local copies, waits for them, and re-layouts: 1.97 us -> 0.84 us
    pallas_call x1, Pallas kernels: 36.7 us -> 34.1 us  [on_line(): pl.pallas_call(mixing_kernel, out_shape=jax.ShapeDtypeStruct((length, fea...]
    unnamed x1, local copies, waits for them, and re-layouts: 1.97 us -> 0.84 us
where the time goes in v3:
time: 35.1 us; the launch traced here: 35 us
  Pallas kernels  34.1 us (97%)
  local copies, waits for them, and re-layouts  0.84 us (2%)
    pallas_call x1, Pallas kernels, on_line(): pl.pallas_call(mixing_kernel, out_shape=jax.ShapeDtypeStruct((length, fea...  34.1 us
    unnamed x1, local copies, waits for them, and re-layouts  0.84 us

profile of v3, /device:TPU:0, one launch (start us, length us, event | category | flops | bytes accessed | tf_op | source)
XLA Modules:
  0.0 35.0 jit_solution(2177154436719707865)
XLA Ops:
  0.0 34.1 %shard_map.64 = bf16[640,512]{1,0:T(8,128)(2,1)S(1)} custom-call(bf16[640,2048]{1,0:T(8,128)(2,1)} %tokens_hbm.1, bf16[2048,256]{1,0:T(8,128)(2,1)} %four_hbm.1, bf16[2048,512]{1,0:T(8,128)(2,1)} %gate_hbm.1, bf16[1024,512]{1,0:T(8,128)(2,1)} %back_hbm.1, bf16[4,160,1280]{2,1,0:T(8,128)(2,1)} %constant.4.clone.table_hbm, ...), custom_call_target="tpu_custom_call" | custom-call | tf_op jit(solution)/shard_map/pallas_call | solution.py:385
  34.1 0.8 %copy.8 = bf16[640,512]{1,0:T(8,128)(2,1)} copy(bf16[640,512]{1,0:T(8,128)(2,1)S(1)} %shard_map.64) | data formatting | bytes 1310720

commit v4 on v3

--- a/solution.py
+++ b/solution.py
@@ -103,6 +103,7 @@
 
 MESH = pl.DeviceIdType.MESH
 TILE = 160
+PIECE = 128
 
 
 def position_table(length, row_count):
@@ -131,7 +132,7 @@
     row, col = lax.axis_index("row"), lax.axis_index("col")
     length = tokens.shape[0]
     quarter, half = length // 4, length // 2
-    tiles = length // TILE
+    tiles, pieces = length // TILE, length // PIECE
     groups = lines.shape[0]
     scale = 1.0 / math.sqrt(4 * length * GROUP_DIM)
     inner = jnp.logical_or(row == 1, row == 2)
@@ -149,6 +150,9 @@
 
     def tile_rows(tile):
         return pl.ds(pl.multiple_of(tile * TILE, TILE), TILE)
+
+    def piece_rows(piece):
+        return pl.ds(pl.multiple_of(piece * PIECE, PIECE), PIECE)
 
     def token_copy(tile):
         return pltpu.make_async_copy(tokens_hbm.at[tile_rows(tile), :], tokens.at[tile_rows(tile), :], token_sem.at[tile])
@@ -239,7 +243,7 @@
             relay(g)
 
     def outer_copy(g, part):
-        rows = pl.ds(part * half, half)
+        rows = piece_rows(part)
         return pltpu.make_async_remote_copy(
             src_ref=outer.at[g, rows],
             dst_ref=blocks.at[g, 0, rows],
@@ -250,7 +254,7 @@
         )
 
     def col_copy(g, part, source, slot, target):
-        rows = pl.ds(part * half, half)
+        rows = piece_rows(part)
         return pltpu.make_async_remote_copy(
             src_ref=blocks.at[g, source, rows],
             dst_ref=blocks.at[g, slot, rows],
@@ -287,21 +291,23 @@
                 spect[3, low, :] = (sin_of[1] - cos_of[3]).astype(jnp.bfloat16)
 
         for at in range(2):
-            for part in range(2):
-                rows = pl.ds(part * half, half)
-                some = pl.ds(part * quarter // 2, quarter // 2)
+
+            @pl.loop(0, pieces)
+            def _(part):
+                step = PIECE // 4
+                some = pl.ds(pl.multiple_of(part * step, step), step)
                 for s in range(4):
-                    value = dot32(turned[at, s, some, :], spect[s]) * scale
-                    final[at, pl.ds(part * half + s, quarter // 2, stride=4), :] = value
+                    final[pl.ds(s, step, stride=4), :] = dot32(turned[at, s, some, :], spect[s]) * scale
                 if at == 0:
-                    outer[g, rows, :] = final[at, rows, :].astype(jnp.bfloat16)
+                    outer[g, piece_rows(part), :] = final[...].astype(jnp.bfloat16)
                     outer_copy(g, part).start()
                 else:
-                    blocks[g, 0, rows, :] = final[at, rows, :].astype(jnp.bfloat16)
+                    blocks[g, 0, piece_rows(part), :] = final[...].astype(jnp.bfloat16)
                     share_own(g, part)
 
     def receive(g):
-        for part in range(2):
+        @pl.loop(0, pieces)
+        def _(part):
             outer_copy(g, part).wait_recv()
             share_own(g, part)
 
@@ -309,42 +315,34 @@
         return w_back[pl.ds(pl.multiple_of((peer * groups + g) * GROUP_DIM, GROUP_DIM), GROUP_DIM), :]
 
     def out_copy(part):
-        rows = pl.ds(part * half, half)
+        rows = piece_rows(part)
         return pltpu.make_async_copy(ready.at[rows, :], out_hbm.at[rows, :], out_sem.at[part])
 
     def finish(g):
-        for part in range(2):
+        @pl.loop(0, pieces)
+        def _(part):
+            rows = piece_rows(part)
             col_copy(g, part, 0, 1, sibling).wait_recv()
-
-            @pl.loop(part * tiles // 2, (part + 1) * tiles // 2)
-            def _(tile):
-                rows = tile_rows(tile)
-                share = dot32(blocks[g, 0, rows, :], back_rows(g, col))
-                share = share + dot32(blocks[g, 1, rows, :], back_rows(g, sibling))
-                total[rows, :] = share if g == 0 else total[rows, :] + share
-
-        for part in range(2):
+            share = dot32(blocks[g, 0, rows, :], back_rows(g, col))
+            share = share + dot32(blocks[g, 1, rows, :], back_rows(g, sibling))
+            total[rows, :] = share if g == 0 else total[rows, :] + share
+
+        @pl.loop(0, pieces)
+        def _(part):
+            rows = piece_rows(part)
             col_copy(g, part, 0, 2, across).wait_recv()
             col_copy(g, part, 2, 3, sibling).start()
-
-            @pl.loop(part * tiles // 2, (part + 1) * tiles // 2)
-            def _(tile):
-                rows = tile_rows(tile)
-                total[rows, :] += dot32(blocks[g, 2, rows, :], back_rows(g, across))
-
-        for part in range(2):
+            total[rows, :] += dot32(blocks[g, 2, rows, :], back_rows(g, across))
+
+        @pl.loop(0, pieces)
+        def _(part):
+            rows = piece_rows(part)
             col_copy(g, part, 2, 3, sibling).wait_recv()
-
-            @pl.loop(part * tiles // 2, (part + 1) * tiles // 2)
-            def _(tile):
-                rows = tile_rows(tile)
-                summed = total[rows, :] + dot32(blocks[g, 3, rows, :], back_rows(g, opposite))
-                if g < groups - 1:
-                    total[rows, :] = summed
-                else:
-                    ready[rows, :] = (gate[rows, :] * summed).astype(jnp.bfloat16)
-
-            if g == groups - 1:
+            summed = total[rows, :] + dot32(blocks[g, 3, rows, :], back_rows(g, opposite))
+            if g < groups - 1:
+                total[rows, :] = summed
+            else:
+                ready[rows, :] = (gate[rows, :] * summed).astype(jnp.bfloat16)
                 out_copy(part).start()
 
     @pl.when(inner)
@@ -358,29 +356,38 @@
 
     for part in range(2):
         for g in range(groups):
+            line_copy(g, part, row, own_target, 0).wait_send()
+
+    @pl.loop(0, pieces)
+    def _(part):
+        for g in range(groups):
             for slot in (1, 2, 3):
                 col_copy(g, part, 0 if slot < 3 else 2, slot, sibling).wait_send()
-            line_copy(g, part, row, own_target, 0).wait_send()
-    for part in range(2):
-
-        @pl.when(inner)
-        def _():
+        out_copy(part).wait()
+
+    @pl.when(inner)
+    def _():
+        for part in range(2):
+            for g in range(groups):
+                line_copy(g, part, end_row, 3 - row, 1).wait_send()
+
+        @pl.loop(0, pieces)
+        def _(part):
             for g in range(groups):
                 outer_copy(g, part).wait_send()
-                line_copy(g, part, end_row, 3 - row, 1).wait_send()
-
-        out_copy(part).wait()
 
 
 def on_line(tokens, w_four, w_gate, w_back):
     length, width = tokens.shape
     groups = w_four.shape[1] // GROUP_DIM
     features = w_gate.shape[1]
-    quarter = length // 4
+    pieces = length // PIECE
     low = jnp.bfloat16
     table = jnp.asarray(position_table(length, 4))
     group = jnp.asarray(group_table())
-    tokens, w_four, w_gate, w_back, table, group = (pltpu.with_memory_space_constraint(x, pltpu.HBM) for x in (tokens, w_four, w_gate, w_back, table, group))
+    tokens, w_four, w_gate, w_back, table, group = (
+        pltpu.with_memory_space_constraint(x, pltpu.HBM) for x in (tokens, w_four, w_gate, w_back, table, group)
+    )
     hbm = pl.BlockSpec(memory_space=pltpu.HBM)
     return pl.pallas_call(
         mixing_kernel,
@@ -397,7 +404,7 @@
             pltpu.VMEM((2,) + table.shape, low),
             pltpu.VMEM((groups, 4, length, GROUP_DIM), low),
             pltpu.VMEM((4, 2 * length, GROUP_DIM), low),
-            pltpu.VMEM((2, length, GROUP_DIM), jnp.float32),
+            pltpu.VMEM((PIECE, GROUP_DIM), jnp.float32),
             pltpu.VMEM((groups, 4, length, GROUP_DIM), low),
             pltpu.VMEM((groups, length, GROUP_DIM), low),
             pltpu.VMEM((length, features), jnp.float32),
@@ -407,11 +414,11 @@
             pltpu.SemaphoreType.DMA((length // TILE,)),
             pltpu.SemaphoreType.DMA((2, groups, 2)),
             pltpu.SemaphoreType.DMA((groups, 2, 4)),
-            pltpu.SemaphoreType.DMA((groups, 2)),
-            pltpu.SemaphoreType.DMA((groups, 2)),
-            pltpu.SemaphoreType.DMA((groups, 2, 4)),
-            pltpu.SemaphoreType.DMA((groups, 2, 4)),
-            pltpu.SemaphoreType.DMA((2,)),
+            pltpu.SemaphoreType.DMA((groups, pieces)),
+            pltpu.SemaphoreType.DMA((groups, pieces)),
+            pltpu.SemaphoreType.DMA((groups, pieces, 4)),
+            pltpu.SemaphoreType.DMA((groups, pieces, 4)),
+            pltpu.SemaphoreType.DMA((pieces,)),
         ],
         compiler_params=pltpu.CompilerParams(
             collective_id=0, has_side_effects=True, vmem_limit_bytes=28 * 1024 * 1024

time: 35.1 us -> 35.5 us (1.011)
  Pallas kernels: 34.1 us -> 34.5 us
where the time goes in v4:
time: 35.5 us; the launch traced here: 35.3 us
  Pallas kernels  34.5 us (97%)
  local copies, waits for them, and re-layouts  0.84 us (2%)
    pallas_call x1, Pallas kernels, on_line(): pl.pallas_call(mixing_kernel, out_shape=jax.ShapeDtypeStruct((length, fea...  34.5 us
    unnamed x1, local copies, waits for them, and re-layouts  0.84 us

profile of v4, /device:TPU:0, one launch (start us, length us, event | category | flops | bytes accessed | tf_op | source)
XLA Modules:
  0.0 35.3 jit_solution(9032374015898243366)
XLA Ops:
  0.0 34.5 %shard_map.64 = bf16[640,512]{1,0:T(8,128)(2,1)S(1)} custom-call(bf16[640,2048]{1,0:T(8,128)(2,1)} %tokens_hbm.1, bf16[2048,256]{1,0:T(8,128)(2,1)} %four_hbm.1, bf16[2048,512]{1,0:T(8,128)(2,1)} %gate_hbm.1, bf16[1024,512]{1,0:T(8,128)(2,1)} %back_hbm.1, bf16[4,160,1280]{2,1,0:T(8,128)(2,1)} %constant.4.clone.table_hbm, ...), custom_call_target="tpu_custom_call" | custom-call | tf_op jit(solution)/shard_map/pallas_call | solution.py:392
  34.5 0.8 %copy.8 = bf16[640,512]{1,0:T(8,128)(2,1)} copy(bf16[640,512]{1,0:T(8,128)(2,1)S(1)} %shard_map.64) | data formatting | bytes 1310720
